TPU v7x, 32 devices: a whole 2x2x4 slice. The times are simulated.
32 devices in a mesh: fs: 4 (over z), rep: 4 (over y, x), tp: 2 (over core).
Axes of the slice: x: 2, y: 2, z: 4, core: 2. Of those that a mesh axis runs over, the one named last changes fastest.
Arguments:
- saved_in: bfloat16 [4096, 4096], P(('fs', 'rep', 'tp')), may hold values from -6 to 6
- out_cot: bfloat16 [4096, 4096], P(('fs', 'rep', 'tp')), may hold values from -0.09375 to 0.09375
- value_cot: bfloat16 [4096, 2048], P(('fs', 'rep'), 'tp'), may hold values from -0.09375 to 0.09375
- mixed_out: bfloat16 [4096, 2048], P(('fs', 'rep'), 'tp'), may hold values from -6 to 6
- value_factor: bfloat16 [4096, 512], P('fs'), may hold values from -0.09375 to 0.09375
- out_factor: bfloat16 [4096, 512], P('fs'), may hold values from -0.09375 to 0.09375
- value_weight: float32 [4096, 2048], P('fs', 'tp'), may hold values from -0.09375 to 0.09375
- out_weight: float32 [2048, 4096], P('tp', 'fs'), may hold values from -0.125 to 0.125
- value_first: float32 [512, 2048], P('fs', 'tp'), may hold values from -6 to 6
- value_second: float32 [512, 2048], P('fs', 'tp'), may hold values from 0.25 to 4
- out_first: float32 [512, 2048], P('fs', 'tp'), may hold values from -6 to 6
- out_second: float32 [512, 2048], P('fs', 'tp'), may hold values from 0.25 to 4
Outputs:
- value_weight_new: float32 [4096, 2048], P('fs', 'tp')
- value_weight_copy: bfloat16 [4096, 2048], P('fs', 'tp')
- out_weight_new: float32 [2048, 4096], P('tp', 'fs')
- out_weight_copy: bfloat16 [2048, 4096], P('tp', 'fs')
- value_first_new: float32 [512, 2048], P('fs', 'tp')
- value_second_new: float32 [512, 2048], P('fs', 'tp')
- out_first_new: float32 [512, 2048], P('fs', 'tp')
- out_second_new: float32 [512, 2048], P('fs', 'tp')
- value_step: float32 [512, 2048], P('fs', 'tp')
- out_step: float32 [512, 2048], P('fs', 'tp')
All inputs are finite; a program needn't handle non-finite values.
Results may differ from a plain program's by a relative error of at most 0.005.
Values may be sent and summed in bfloat16 or wider, within the bound.
A program may use at most 128 MiB of HBM per device.

v0:
```python
import jax
import jax.numpy as jnp
from jax import lax
from jax.sharding import PartitionSpec as P

CHANNELS = 2048
RANK = 512
beta_first = 0.8
beta_second = 0.9
step_rate = 0.05
clip_level = 0.5


def fold_pair(left_in, left_cot, pieces):
    return (
        jnp.dot(left_in, pieces[0], preferred_element_type=jnp.float32),
        jnp.dot(left_cot, pieces[1], preferred_element_type=jnp.float32),
    )


def contract_rows(left, right):
    return lax.dot_general(
        left, right, (((0,), (0,)), ((), ())), preferred_element_type=jnp.float32
    )


def adapt(grad, first, second):
    new_first = beta_first * first + (1.0 - beta_first) * grad
    new_second = beta_second * second + (1.0 - beta_second) * grad * grad
    lowered = (new_first / jnp.sqrt(new_second)).astype(jnp.bfloat16)
    return (new_first, new_second, lowered)


def shards(
    saved_in,
    out_cot,
    value_cot,
    mixed_out,
    value_factor,
    out_factor,
    value_weight,
    out_weight,
    value_first,
    value_second,
    out_first,
    out_second,
):
    rank_cols = value_factor.shape[1]
    half_width = rank_cols // 2
    offset = lax.axis_index("tp") * half_width
    half_value = lax.dynamic_slice_in_dim(value_factor, offset, half_width, 1)
    half_out = lax.dynamic_slice_in_dim(out_factor, offset, half_width, 1)
    both_in, both_cot = (
        lax.all_gather(saved_in, "tp", axis=0, tiled=True),
        lax.all_gather(out_cot, "tp", axis=0, tiled=True),
    )
    proj_in, proj_cot = fold_pair(
        both_in,
        both_cot,
        (
            lax.all_gather(half_value, "fs", axis=0, tiled=True),
            lax.all_gather(half_out, "fs", axis=0, tiled=True),
        ),
    )
    proj_in, proj_cot = (
        lax.all_gather(proj_in.astype(jnp.bfloat16), "tp", axis=1, tiled=True),
        lax.all_gather(proj_cot.astype(jnp.bfloat16), "tp", axis=1, tiled=True),
    )
    summed = lax.psum_scatter(
        jnp.concatenate(
            [contract_rows(proj_in, value_cot), contract_rows(proj_cot, mixed_out)], axis=1
        ),
        "fs",
        scatter_dimension=0,
        tiled=True,
    )
    summed = lax.psum(summed.astype(jnp.bfloat16), "rep").astype(jnp.float32)
    chan_cols = value_cot.shape[1]
    value_first_new, value_second_new, low_value = adapt(
        summed[:, :chan_cols], value_first, value_second
    )
    out_first_new, out_second_new, low_out = adapt(summed[:, chan_cols:], out_first, out_second)
    lowered = jnp.concatenate([low_value, low_out], axis=1)
    gathered = lax.all_gather(lowered, "fs", axis=0, tiled=True)
    own_float = lowered.astype(jnp.float32)
    total = lax.psum(jnp.sum(own_float * own_float), ("fs", "tp"))
    spread = jnp.sqrt(total / (2.0 * RANK * CHANNELS))
    scale = clip_level / jnp.maximum(spread, clip_level)
    value_full = jnp.dot(value_factor, gathered[:, :chan_cols], preferred_element_type=jnp.float32)
    out_full = lax.dot_general(
        gathered[:, chan_cols:],
        out_factor,
        (((0,), (1,)), ((), ())),
        preferred_element_type=jnp.float32,
    )
    value_weight_new = value_weight - step_rate * scale * value_full
    out_weight_new = out_weight - step_rate * scale * out_full
    return (
        value_weight_new,
        value_weight_new.astype(jnp.bfloat16),
        out_weight_new,
        out_weight_new.astype(jnp.bfloat16),
        value_first_new,
        value_second_new,
        out_first_new,
        out_second_new,
        scale * low_value.astype(jnp.float32),
        scale * low_out.astype(jnp.float32),
    )


def solution(mesh):
    placed = (
        P(("fs", "rep", "tp"), None),
        P(("fs", "rep", "tp"), None),
        P(("fs", "rep"), "tp"),
        P(("fs", "rep"), "tp"),
        P("fs", None),
        P("fs", None),
        P("fs", "tp"),
        P("tp", "fs"),
        P("fs", "tp"),
        P("fs", "tp"),
        P("fs", "tp"),
        P("fs", "tp"),
    )
    return jax.shard_map(
        shards,
        mesh=mesh,
        in_specs=placed,
        out_specs=(
            P("fs", "tp"),
            P("fs", "tp"),
            P("tp", "fs"),
            P("tp", "fs"),
            P("fs", "tp"),
            P("fs", "tp"),
            P("fs", "tp"),
            P("fs", "tp"),
            P("fs", "tp"),
            P("fs", "tp"),
        ),
        check_vma=False,
    )
```

profile of v0, /device:TPU:0, one launch (start us, length us, event | category | flops | bytes accessed | tf_op | source)
XLA Modules:
  0.0 343.5 jit_solution(9463912163922284512)
XLA Ops:
  8.0 1.9 constant_dynamic-slice_fusion
  11.6 11.3 %all-gather.12.cloned.1.call-done = bf16[256,4096]{1,0:T(8,128)(2,1)} async-done(((bf16[128,4096]{1,0:T(8,128)(2,1)}), bf16[256,4096]{1,0:T(8,128)(2,1)}) %all-gather.12.cloned.1.call-update) | async-done | bytes 2097168 | tf_op jit(solution)/shard_map/all_gather | solution.py:55
  22.9 49.0 %all-gather.10.cloned.1.call-done = bf16[4096,256]{1,0:T(8,128)(2,1)} async-done(((bf16[1024,256]{1,0:T(8,128)(2,1)}), bf16[4096,256]{1,0:T(8,128)(2,1)}) %all-gather.10.cloned.1.call-update) | async-done | bytes 2097168 | tf_op jit(solution)/shard_map/all_gather | solution.py:62
  71.9 3.0 fusion.1
  74.9 2.0 all_gather.26
  76.9 6.0 %all-gather.8.cloned.1.call-done = bf16[256,4096]{1,0:T(8,128)(2,1)} async-done(((bf16[128,4096]{1,0:T(8,128)(2,1)}), bf16[256,4096]{1,0:T(8,128)(2,1)}) %all-gather.8.cloned.1.call-update) | async-done | bytes 2097168 | tf_op jit(solution)/shard_map/all_gather | solution.py:54
  82.8 48.9 %all-gather.6.cloned.1.call-done = bf16[4096,256]{1,0:T(8,128)(2,1)} async-done(((bf16[1024,256]{1,0:T(8,128)(2,1)}), bf16[4096,256]{1,0:T(8,128)(2,1)}) %all-gather.6.cloned.1.call-update) | async-done | bytes 2097168 | tf_op jit(solution)/shard_map/all_gather | solution.py:61
  131.7 3.0 fusion
  134.7 2.1 all_gather.23
  137.7 2.5 pad_maximum_fusion
  140.3 75.7 %reduce-scatter.2.cloned.1.call-done = f32[128,2048]{1,0:T(8,128)} async-done(((f32[512,2048]{1,0:T(8,128)}), f32[128,2048]{1,0:T(8,128)}) %reduce-scatter.2.cloned.1.call-update) | async-done | bytes 1048592 | tf_op jit(solution)/shard_map/reduce_scatter | solution.py:69
  216.0 2.1 convert_element_type.43
  218.2 47.2 %all-reduce.2.cloned.1.call-done = bf16[128,2048]{1,0:T(8,128)(2,1)} async-done(((bf16[128,2048]{1,0:T(8,128)(2,1)}), bf16[128,2048]{1,0:T(8,128)(2,1)}) %all-reduce.2.cloned.1.call-update) | async-done | bytes 524304 | tf_op jit(solution)/shard_map/psum | solution.py:77
  265.3 1.1 convert_element_type.44
  266.5 2.6 multiply_convert_fusion.1
  270.0 0.9 multiply_reduce_fusion
  270.9 5.3 %copy.22 = f32[1024,1024]{0,1:T(8,128)} copy(f32[1024,1024]{1,0:T(8,128)} %param.18) | data formatting | bytes 8388608 | tf_op args[6]
  276.2 17.6 %psum.15 = f32[]{:T(128)} all-reduce(f32[]{:T(128)} %multiply_reduce_fusion), channel_id=1, replica_groups=mesh['fs'=4,'rep'=4,'tp'=2] {'fs','tp'}, use_global_device_ids=true, to_apply=%region_3.0 | all-reduce | flops 1 | bytes 8 | tf_op jit(solution)/shard_map/psum | solution.py:86
  294.6 1.1 convert_multiply_fusion
  295.7 20.4 %all-gather.14.cloned.1.call-done = bf16[512,2048]{1,0:T(8,128)(2,1)} async-done(((bf16[128,2048]{1,0:T(8,128)(2,1)}), bf16[512,2048]{1,0:T(8,128)(2,1)}) %all-gather.14.cloned.1.call-update) | async-done | bytes 2097168 | tf_op jit(solution)/shard_map/all_gather | solution.py:84
  316.1 5.8 %fusion.8 = (bf16[1024,1024]{0,1:T(8,128)(2,1)S(1)}, f32[1024,1024]{0,1:T(8,128)}) fusion(f32[1024,1024]{0,1:T(8,128)} %copy.22, bf16[1024,512]{1,0:T(8,128)(2,1)S(1)} %copy-done, bf16[512,2048]{1,0:T(8,128)(2,1)} %all-gather.14.cloned.1.call-done, f32[]{:T(128)S(6)} %mul.75), kind=kOutput, calls=%fused_computation.23 | convolution fusion | flops 1076887552 | bytes 12582916 | tf_op jit(solution)/shard_map/dot_general | solution.py:89
  321.9 5.3 %copy.23 = f32[1024,1024]{1,0:T(8,128)} copy(f32[1024,1024]{0,1:T(8,128)} %get-tuple-element.30) | data formatting | bytes 8388608
  327.3 2.5 copy.24
  329.8 6.8 %fusion.9 = (bf16[1024,1024]{1,0:T(8,128)(2,1)}, f32[1024,1024]{1,0:T(8,128)}) fusion(f32[1024,1024]{1,0:T(8,128)} %param.19, bf16[1024,512]{1,0:T(8,128)(2,1)} %param.17, bf16[512,2048]{1,0:T(8,128)(2,1)} %all-gather.14.cloned.1.call-done, f32[]{:T(128)S(6)} %mul.75), kind=kOutput, calls=%fused_computation.24 | convolution fusion | flops 1076887552 | bytes 12582916 | tf_op jit(solution)/shard_map/dot_general | solution.py:90
  (30 shorter events, 4.3 us)
Async XLA Ops:
  7.2 3.5 %copy-start = (bf16[1024,512]{1,0:T(8,128)(2,1)S(1)}, bf16[1024,512]{1,0:T(8,128)(2,1)}, u32[]{:S(2)}) copy-start(bf16[1024,512]{1,0:T(8,128)(2,1)} %param.16) | copy-start | bytes 3145732
  7.2 15.7 %all-gather.12.cloned.1.call-start = ((), (), s32[]{:S(2)}) async-start(), calls=%async_computation.4 | async-start | bytes 3145728 | tf_op jit(solution)/shard_map/all_gather | solution.py:55
  7.9 64.0 %all-gather.10.cloned.1.call-start = ((), (), s32[]{:S(2)}) async-start(), calls=%async_computation.3 | async-start | bytes 2621440 | tf_op jit(solution)/shard_map/all_gather | solution.py:62
  9.9 73.0 %all-gather.8.cloned.1.call-start = ((), (), s32[]{:S(2)}) async-start(), calls=%async_computation.2 | async-start | bytes 3145728 | tf_op jit(solution)/shard_map/all_gather | solution.py:54
  10.6 121.1 %all-gather.6.cloned.1.call-start = ((), (), s32[]{:S(2)}) async-start(), calls=%async_computation.1 | async-start | bytes 2621440 | tf_op jit(solution)/shard_map/all_gather | solution.py:61
  11.5 204.5 %reduce-scatter.2.cloned.1.call-start = ((), (), s32[]{:S(2)}) async-start(), calls=%async_computation.5 | async-start | bytes 5242880 | tf_op jit(solution)/shard_map/reduce_scatter | solution.py:69
  76.9 60.0 %copy-start.1 = (bf16[256,1024]{1,0:T(8,128)(2,1)S(1)}, bf16[256,1024]{1,0:T(8,128)(2,1)}, u32[]{:S(2)}) copy-start(bf16[256,1024]{1,0:T(8,128)(2,1)} %param.15) | copy-start | bytes 1572868
  134.7 2.6 copy-start.2
  140.3 126.2 %copy-start.3 = (f32[128,1024]{1,0:T(8,128)S(1)}, f32[128,1024]{1,0:T(8,128)}, u32[]{:S(2)}) copy-start(f32[128,1024]{1,0:T(8,128)} %param.21) | copy-start | bytes 1572868
  140.3 126.2 %copy-start.4 = (f32[128,1024]{1,0:T(8,128)S(1)}, f32[128,1024]{1,0:T(8,128)}, u32[]{:S(2)}) copy-start(f32[128,1024]{1,0:T(8,128)} %param.20) | copy-start | bytes 1572868
  140.3 126.2 %copy-start.5 = (f32[128,1024]{1,0:T(8,128)S(1)}, f32[128,1024]{1,0:T(8,128)}, u32[]{:S(2)}) copy-start(f32[128,1024]{1,0:T(8,128)} %param.23) | copy-start | bytes 1572868
  140.3 125.0 %all-reduce.2.cloned.1.call-start = ((), (), s32[]{:S(2)}) async-start(), calls=%async_computation.6 | async-start | bytes 1048576 | tf_op jit(solution)/shard_map/psum | solution.py:77
  218.1 98.0 %all-gather.14.cloned.1.call-start = ((), (), s32[]{:S(2)}) async-start(), calls=%async_computation.7 | async-start | bytes 2621440 | tf_op jit(solution)/shard_map/all_gather | solution.py:84
Sparse Core Ops, SparseCore 0:
  9.5 13.2 all-gather.11
  25.0 46.8 all-gather.9
  73.4 9.3 all-gather.7
  84.8 46.8 all-gather.5
  140.4 75.5 reduce-scatter.1
  219.4 45.8 all-reduce.1
  270.1 45.9 all-gather.13
where the time goes:
time: 344 us; the launch traced here: 343 us
  waiting for transfers between devices  260 us (76%)
  blocking collectives  21.8 us (6%)
  matrix products  19.5 us (6%)
  local copies, waits for them, and re-layouts  16 us (5%)
  between operations  15 us (4%)
  other arithmetic  11.1 us (3%)
    reduce_scatter x1, waiting for transfers between devices, shards(): lax.psum_scatter(jnp.concatenate([contract_rows(proj_in, value_cot), cont...  75.7 us
    all_gather x1, waiting for transfers between devices, shards(): lax.all_gather(half_out, 'fs', axis=0, tiled=True)  49 us
    all_gather x1, waiting for transfers between devices, shards(): lax.all_gather(half_value, 'fs', axis=0, tiled=True)  48.9 us
    psum x1, waiting for transfers between devices, shards(): summed = lax.psum(summed.astype(jnp.bfloat16), 'rep').astype(jnp.float32)  47.2 us
    all_gather x1, waiting for transfers between devices, shards(): gathered = lax.all_gather(lowered, 'fs', axis=0, tiled=True)  20.4 us
    psum x1, blocking collectives, shards(): total = lax.psum(jnp.sum(own_float * own_float), ('fs', 'tp'))  17.6 us
    unnamed x15, local copies, waits for them, and re-layouts  13.3 us
    all_gather x1, waiting for transfers between devices, shards(): lax.all_gather(out_cot, 'tp', axis=0, tiled=True)  11.3 us
  transfers between devices with their start and end apart: 7, of which 7 were waited for; matrix products, arithmetic and copies ran while one was open for 4% of the time, Pallas kernels for 0%

commit v1 on v0

--- a/solution.py
+++ b/solution.py
@@ -74,7 +74,7 @@
         scatter_dimension=0,
         tiled=True,
     )
-    summed = lax.psum(summed.astype(jnp.bfloat16), "rep").astype(jnp.float32)
+    summed = jnp.sum(lax.all_gather(summed.astype(jnp.bfloat16), "rep"), axis=0).astype(jnp.float32)
     chan_cols = value_cot.shape[1]
     value_first_new, value_second_new, low_value = adapt(
         summed[:, :chan_cols], value_first, value_second

time: 344 us -> 334 us (0.971)
  waiting for transfers between devices: 260 us -> 248 us
    psum x1 -> x0, waiting for transfers between devices: 47.2 us -> none  [shards(): summed = lax.psum(summed.astype(jnp.bfloat16), 'rep').astype(jnp.float32)]
    all_gather x0 -> x1, waiting for transfers between devices: none -> 35.8 us  [shards(): lax.all_gather(summed.astype(jnp.bfloat16), 'rep')]
where the time goes in v1:
time: 334 us; the launch traced here: 333 us
  waiting for transfers between devices  248 us (74%)
  blocking collectives  22.1 us (7%)
  matrix products  19.5 us (6%)
  local copies, waits for them, and re-layouts  16 us (5%)
  between operations  15 us (4%)
  other arithmetic  12.3 us (4%)
    reduce_scatter x1, waiting for transfers between devices, shards(): lax.psum_scatter(jnp.concatenate([contract_rows(proj_in, value_cot), cont...  75.7 us
    all_gather x1, waiting for transfers between devices, shards(): lax.all_gather(half_out, 'fs', axis=0, tiled=True)  49 us
    all_gather x1, waiting for transfers between devices, shards(): lax.all_gather(half_value, 'fs', axis=0, tiled=True)  48.9 us
    all_gather x1, waiting for transfers between devices, shards(): lax.all_gather(summed.astype(jnp.bfloat16), 'rep')  35.8 us
    all_gather x1, waiting for transfers between devices, shards(): gathered = lax.all_gather(lowered, 'fs', axis=0, tiled=True)  20 us
    psum x1, blocking collectives, shards(): total = lax.psum(jnp.sum(own_float * own_float), ('fs', 'tp'))  18 us
    unnamed x15, local copies, waits for them, and re-layouts  13.2 us
    all_gather x1, waiting for transfers between devices, shards(): lax.all_gather(out_cot, 'tp', axis=0, tiled=True)  11.3 us
  transfers between devices with their start and end apart: 7, of which 7 were waited for; matrix products, arithmetic and copies ran while one was open for 4% of the time, Pallas kernels for 0%

profile of v1, /device:TPU:0, one launch (start us, length us, event | category | flops | bytes accessed | tf_op | source)
XLA Modules:
  0.0 333.3 jit_solution(15732721290030254099)
XLA Ops:
  8.0 1.9 constant_dynamic-slice_fusion
  11.6 11.3 %all-gather.14.cloned.1.call-done = bf16[256,4096]{1,0:T(8,128)(2,1)} async-done(((bf16[128,4096]{1,0:T(8,128)(2,1)}), bf16[256,4096]{1,0:T(8,128)(2,1)}) %all-gather.14.cloned.1.call-update) | async-done | bytes 2097168 | tf_op jit(solution)/shard_map/all_gather | solution.py:55
  22.9 49.0 %all-gather.12.cloned.1.call-done = bf16[4096,256]{1,0:T(8,128)(2,1)} async-done(((bf16[1024,256]{1,0:T(8,128)(2,1)}), bf16[4096,256]{1,0:T(8,128)(2,1)}) %all-gather.12.cloned.1.call-update) | async-done | bytes 2097168 | tf_op jit(solution)/shard_map/all_gather | solution.py:62
  71.9 3.0 fusion.1
  74.9 2.0 all_gather.32
  76.9 6.0 %all-gather.10.cloned.1.call-done = bf16[256,4096]{1,0:T(8,128)(2,1)} async-done(((bf16[128,4096]{1,0:T(8,128)(2,1)}), bf16[256,4096]{1,0:T(8,128)(2,1)}) %all-gather.10.cloned.1.call-update) | async-done | bytes 2097168 | tf_op jit(solution)/shard_map/all_gather | solution.py:54
  82.8 48.9 %all-gather.8.cloned.1.call-done = bf16[4096,256]{1,0:T(8,128)(2,1)} async-done(((bf16[1024,256]{1,0:T(8,128)(2,1)}), bf16[4096,256]{1,0:T(8,128)(2,1)}) %all-gather.8.cloned.1.call-update) | async-done | bytes 2097168 | tf_op jit(solution)/shard_map/all_gather | solution.py:61
  131.7 3.0 fusion
  134.7 2.1 all_gather.29
  137.7 2.5 pad_maximum_fusion
  140.3 75.7 %reduce-scatter.2.cloned.1.call-done = f32[128,2048]{1,0:T(8,128)} async-done(((f32[512,2048]{1,0:T(8,128)}), f32[128,2048]{1,0:T(8,128)}) %reduce-scatter.2.cloned.1.call-update) | async-done | bytes 1048592 | tf_op jit(solution)/shard_map/reduce_scatter | solution.py:69
  216.0 2.1 convert_element_type.45
  218.2 35.8 %all-gather.18.cloned.1.call-done = bf16[512,2048]{1,0:T(8,128)(2,1)} async-done(((bf16[128,2048]{1,0:T(8,128)(2,1)}), bf16[512,2048]{1,0:T(8,128)(2,1)}) %all-gather.18.cloned.1.call-update) | async-done | bytes 2097168 | tf_op jit(solution)/shard_map/all_gather | solution.py:77
  254.0 2.1 reduce_sum.21
  256.3 2.6 multiply_convert_fusion.1
  259.8 0.9 multiply_reduce_fusion
  260.7 5.3 %copy.22 = f32[1024,1024]{0,1:T(8,128)} copy(f32[1024,1024]{1,0:T(8,128)} %param.18) | data formatting | bytes 8388608 | tf_op args[6]
  266.0 18.0 %psum.7 = f32[]{:T(128)} all-reduce(f32[]{:T(128)} %multiply_reduce_fusion), channel_id=1, replica_groups=mesh['fs'=4,'rep'=4,'tp'=2] {'fs','tp'}, use_global_device_ids=true, to_apply=%region_3.0 | all-reduce | flops 1 | bytes 8 | tf_op jit(solution)/shard_map/psum | solution.py:86
  284.7 1.1 convert_multiply_fusion
  285.8 20.0 %all-gather.16.cloned.1.call-done = bf16[512,2048]{1,0:T(8,128)(2,1)} async-done(((bf16[128,2048]{1,0:T(8,128)(2,1)}), bf16[512,2048]{1,0:T(8,128)(2,1)}) %all-gather.16.cloned.1.call-update) | async-done | bytes 2097168 | tf_op jit(solution)/shard_map/all_gather | solution.py:84
  305.9 5.8 %fusion.8 = (bf16[1024,1024]{0,1:T(8,128)(2,1)S(1)}, f32[1024,1024]{0,1:T(8,128)}) fusion(f32[1024,1024]{0,1:T(8,128)} %copy.22, bf16[1024,512]{1,0:T(8,128)(2,1)S(1)} %copy-done, bf16[512,2048]{1,0:T(8,128)(2,1)} %all-gather.16.cloned.1.call-done, f32[]{:T(128)S(6)} %mul.75), kind=kOutput, calls=%fused_computation.23 | convolution fusion | flops 1076887552 | bytes 12582916 | tf_op jit(solution)/shard_map/dot_general | solution.py:89
  311.7 5.3 %copy.23 = f32[1024,1024]{1,0:T(8,128)} copy(f32[1024,1024]{0,1:T(8,128)} %get-tuple-element.30) | data formatting | bytes 8388608
  317.0 2.5 copy.24
  319.6 6.8 %fusion.9 = (bf16[1024,1024]{1,0:T(8,128)(2,1)}, f32[1024,1024]{1,0:T(8,128)}) fusion(f32[1024,1024]{1,0:T(8,128)} %param.19, bf16[1024,512]{1,0:T(8,128)(2,1)} %param.17, bf16[512,2048]{1,0:T(8,128)(2,1)} %all-gather.16.cloned.1.call-done, f32[]{:T(128)S(6)} %mul.75), kind=kOutput, calls=%fused_computation.24 | convolution fusion | flops 1076887552 | bytes 12582916 | tf_op jit(solution)/shard_map/dot_general | solution.py:90
  (31 shorter events, 4.4 us)
Async XLA Ops:
  7.2 3.5 %copy-start = (bf16[1024,512]{1,0:T(8,128)(2,1)S(1)}, bf16[1024,512]{1,0:T(8,128)(2,1)}, u32[]{:S(2)}) copy-start(bf16[1024,512]{1,0:T(8,128)(2,1)} %param.16) | copy-start | bytes 3145732
  7.2 15.7 %all-gather.14.cloned.1.call-start = ((), (), s32[]{:S(2)}) async-start(), calls=%async_computation.4 | async-start | bytes 3145728 | tf_op jit(solution)/shard_map/all_gather | solution.py:55
  7.9 64.0 %all-gather.12.cloned.1.call-start = ((), (), s32[]{:S(2)}) async-start(), calls=%async_computation.3 | async-start | bytes 2621440 | tf_op jit(solution)/shard_map/all_gather | solution.py:62
  9.9 73.0 %all-gather.10.cloned.1.call-start = ((), (), s32[]{:S(2)}) async-start(), calls=%async_computation.2 | async-start | bytes 3145728 | tf_op jit(solution)/shard_map/all_gather | solution.py:54
  10.6 121.1 %all-gather.8.cloned.1.call-start = ((), (), s32[]{:S(2)}) async-start(), calls=%async_computation.1 | async-start | bytes 2621440 | tf_op jit(solution)/shard_map/all_gather | solution.py:61
  11.5 204.5 %reduce-scatter.2.cloned.1.call-start = ((), (), s32[]{:S(2)}) async-start(), calls=%async_computation.5 | async-start | bytes 5242880 | tf_op jit(solution)/shard_map/reduce_scatter | solution.py:69
  76.9 60.0 %copy-start.1 = (bf16[256,1024]{1,0:T(8,128)(2,1)S(1)}, bf16[256,1024]{1,0:T(8,128)(2,1)}, u32[]{:S(2)}) copy-start(bf16[256,1024]{1,0:T(8,128)(2,1)} %param.15) | copy-start | bytes 1572868
  134.7 2.6 copy-start.2
  140.3 113.8 %all-gather.18.cloned.1.call-start = ((), (), s32[]{:S(2)}) async-start(), calls=%async_computation.7 | async-start | bytes 2621440 | tf_op jit(solution)/shard_map/all_gather | solution.py:77
  218.1 87.8 %all-gather.16.cloned.1.call-start = ((), (), s32[]{:S(2)}) async-start(), calls=%async_computation.6 | async-start | bytes 2621440 | tf_op jit(solution)/shard_map/all_gather | solution.py:84
  254.0 2.3 copy-start.3
  254.0 2.3 copy-start.4
  254.0 2.3 copy-start.5
Sparse Core Ops, SparseCore 0:
  9.5 13.2 all-gather.13
  25.0 46.8 all-gather.11
  73.4 9.3 all-gather.9
  84.8 46.8 all-gather.7
  140.4 75.5 reduce-scatter.1
  218.3 35.6 all-gather.17
  259.9 45.9 all-gather.15
